TPU v7x, 512 devices: a whole 4x4x16 slice. The times are simulated.
512 devices in a mesh: pp: 16 (over y, x), tp: 32 (over z, core).
Axes of the slice: x: 4, y: 4, z: 16, core: 2. Of those that a mesh axis runs over, the one named last changes fastest.
Arguments:
- entry_stream_rows: bfloat16 [1024, 2048], P('pp', 'tp'), may hold values from -21 to 21
- layer_rescale_factor: float32 [16, 2048], P('pp'), may hold values from 0.1 to 1.9
- probe_projection: bfloat16 [16, 2048, 2048], P('pp', 'tp'), may hold values from -0.125 to 0.125
- retention_projection: bfloat16 [16, 2048, 2048], P('pp', 'tp'), may hold values from -0.125 to 0.125
- candidate_projection: bfloat16 [16, 2048, 2048], P('pp', 'tp'), may hold values from -0.125 to 0.125
- emission_filter_matrix: bfloat16 [16, 2048, 2048], P('pp', 'tp'), may hold values from -0.125 to 0.125
- retention_minimum: float32 [16, 2048], P('pp', 'tp'), may hold values from 0.88 to 0.9921875
- decay_spike: float32 [16, 128, 32], P('pp', None, 'tp'), may hold values from -2.1 to 0
- per_group_scale: float32 [16, 64], P('pp'), may hold values from 0.1 to 1.9
Outputs:
- outputs: bfloat16 [1024, 2048], P('pp', 'tp')
All inputs are finite; a program needn't handle non-finite values.
Results may differ from a plain program's by a relative error of at most 0.03.
Values may be sent and summed in bfloat16 or wider, within the bound.
No kernel may reach another device: no remote copies, remote signals or barrier semaphores. Data moves between devices by JAX's collectives and lax.ppermute only.
A program may use at most 64 MiB of HBM per device.

v0:
```python
import jax
import jax.numpy as jnp
from jax import lax
from jax.sharding import PartitionSpec as P

HEAD = 64
SEG = 64
EPSILON = 1e-06


def shifted(array, axis, by):
    devices = lax.axis_size(axis)
    pairs = [(i, i + by) for i in range(devices) if 0 <= i + by < devices]
    return lax.ppermute(array, axis, pairs)


def from_root(array, axis, root):
    return lax.dynamic_index_in_dim(lax.all_gather(array, axis), root, 0, keepdims=False)


def segment_scan(queries, key_in, log_forget, values, memory):
    head_count = queries.shape[0]
    length = queries.shape[1]
    blocks_count = length // SEG

    def split_blocks(tensor):
        return tensor.reshape(head_count, blocks_count, SEG, tensor.shape[-1]).transpose(1, 0, 2, 3)

    lower_mask = jnp.tril(jnp.ones((SEG, SEG), dtype=bool))[None]

    def one_block(memory_in, pieces):
        block_query, block_key, block_forget, block_value = pieces
        running = jnp.cumsum(block_forget, axis=1)
        query_scaled = block_query * jnp.exp(running)
        key_scaled = block_key * jnp.exp(-running)
        scores = jnp.einsum("hid,hjd->hij", query_scaled, key_scaled)
        scores = jnp.where(lower_mask, scores, 0.0)
        mixed_out = jnp.einsum("hij,hjv->hiv", scores, block_value)
        mixed_out = mixed_out + jnp.einsum("hid,hdv->hiv", query_scaled, memory_in)
        ending = running[:, -1:, :]
        carried_in = jnp.einsum("hjd,hjv->hdv", block_key * jnp.exp(ending - running), block_value)
        memory_out = jnp.exp(ending[:, 0, :])[:, :, None] * memory_in + carried_in
        return (memory_out, mixed_out)

    memory, mixed_out = lax.scan(
        one_block,
        memory,
        (
            split_blocks(queries),
            split_blocks(key_in),
            split_blocks(log_forget),
            split_blocks(values),
        ),
    )
    return (mixed_out.transpose(1, 0, 2, 3).reshape(head_count, length, values.shape[-1]), memory)


def head_norm(mixed_out, channel_gain):
    return (
        mixed_out
        * lax.rsqrt(jnp.mean(mixed_out * mixed_out, axis=-1, keepdims=True) + EPSILON)
        * channel_gain
    )


def shards(
    entry_stream_rows,
    layer_rescale_factor,
    probe_projection,
    retention_projection,
    candidate_projection,
    emission_filter_matrix,
    retention_minimum,
    decay_spike,
    per_group_scale,
):
    sections = lax.axis_size("pp")
    layer_ordinal = lax.axis_index("pp")
    own_rows = entry_stream_rows.shape[0]
    seq_len = 2 * own_rows
    columns = entry_stream_rows.shape[1]
    head_here = columns // HEAD
    model_width = layer_rescale_factor.shape[1]
    micro_count = sections // 2
    per_sequence = seq_len // seq_len
    unit_count = micro_count * per_sequence
    total_steps = unit_count + sections - 1
    entering = lax.all_gather(entry_stream_rows, "pp", axis=0, tiled=True)
    weights = jnp.concatenate(
        [
            probe_projection[0],
            retention_projection[0],
            candidate_projection[0],
            emission_filter_matrix[0],
        ],
        axis=0,
    )
    input_gain = layer_rescale_factor[0]
    lower_edge = retention_minimum[0].reshape(head_here, 1, HEAD)
    spike_collection = decay_spike[0].T
    out_gain = per_group_scale[0]

    def add_piece(piece_in):
        wide_piece = piece_in.astype(jnp.float32)
        scaled = (wide_piece * input_gain[None, :]).astype(jnp.bfloat16)
        product = lax.dot_general(
            scaled, weights, (((1,), (1,)), ((), ())), preferred_element_type=jnp.float32
        )
        return (product, jnp.sum(wide_piece * wide_piece, axis=1))

    def one_step(step_index, carried):
        incoming, memory, finished = carried
        unit_index = step_index - layer_ordinal
        first_slot = jnp.clip(step_index, 0, unit_count - 1)
        fresh_rows = lax.dynamic_slice_in_dim(entering, first_slot * seq_len, seq_len, 0)
        current = jnp.where(layer_ordinal == 0, fresh_rows, incoming)
        projected, squares = add_piece(lax.all_gather(current, "tp", axis=1, tiled=True))
        inverse = lax.rsqrt(squares / model_width + EPSILON)[:, None]
        projected = projected * inverse

        def per_head(role_index):
            picked = projected[:, role_index * columns : (role_index + 1) * columns]
            return picked.reshape(seq_len, head_here, HEAD).transpose(1, 0, 2)

        query_pre = per_head(0)
        forget_pre = per_head(1)
        input_pre = per_head(2)
        gate_pre = per_head(3)
        offset = unit_index % per_sequence * seq_len
        current_surge = spike_collection[:, :, None]
        log_forget = (
            jnp.logaddexp(
                jnp.log(lower_edge), jnp.log1p(-lower_edge) + jax.nn.log_sigmoid(forget_pre)
            )
            + current_surge
        )
        key_in = (1.0 - lower_edge) * jax.nn.sigmoid(-forget_pre)
        queries = jax.nn.silu(query_pre)
        memory = jnp.where(offset == 0, jnp.zeros_like(memory), memory)
        mixed_out, memory = segment_scan(queries, key_in, log_forget, input_pre, memory)
        branch = head_norm(mixed_out, out_gain) * jax.nn.silu(gate_pre)
        branch = branch.transpose(1, 0, 2).reshape(seq_len, columns)
        result = (current.astype(jnp.float32) + branch).astype(jnp.bfloat16)
        passed = shifted(result, "pp", 1)
        out_slot = jnp.clip(unit_index, 0, unit_count - 1)
        write_here = (layer_ordinal == sections - 1) & (unit_index >= 0) & (unit_index < unit_count)
        updated = lax.dynamic_update_slice_in_dim(finished, result, out_slot * seq_len, 0)
        finished = jnp.where(write_here, updated, finished)
        return (passed, memory, finished)

    start_state = (
        jnp.zeros((seq_len, columns), jnp.bfloat16),
        jnp.zeros((head_here, HEAD, HEAD), jnp.float32),
        jnp.zeros((unit_count * seq_len, columns), jnp.bfloat16),
    )
    carried_out = lax.fori_loop(0, total_steps, one_step, start_state)
    everything = from_root(carried_out[2], "pp", sections - 1)
    return lax.dynamic_slice_in_dim(everything, layer_ordinal * own_rows, own_rows, 0)


def solution(mesh):
    in_specs = (
        P("pp", "tp"),
        P("pp", None),
        P("pp", "tp", None),
        P("pp", "tp", None),
        P("pp", "tp", None),
        P("pp", "tp", None),
        P("pp", "tp"),
        P("pp", None, "tp"),
        P("pp", None),
    )
    out_specs = P("pp", "tp")
    return jax.shard_map(shards, mesh=mesh, in_specs=in_specs, out_specs=out_specs, check_vma=False)
```

profile of v0, /device:TPU:1, one launch (start us, length us, event | category | flops | bytes accessed | tf_op | source)
XLA Modules:
  0.0 1040.1 jit_solution(864880211558230233)
XLA Ops:
  7.3 19.7 %all_gather.20 = bf16[1024,64]{1,0:T(8,128)(2,1)S(1)} all-gather(bf16[64,64]{1,0:T(8,128)(2,1)} %param.13), channel_id=1, replica_groups=mesh['pp'=16,'tp'=32] {'pp'}, dimensions={0}, use_global_device_ids=true | all-gather | bytes 139264 | tf_op jit(solution)/shard_map/all_gather | solution.py:88
  28.3 930.2 %while.59 = (s32[]{:T(128)}, bf16[128,64]{1,0:T(8,128)(2,1)S(1)}, bf16[1024,64]{1,0:T(8,128)(2,1)S(1)}, pred[]{:T(512)}, bf16[1024,64]{1,0:T(8,128)(2,1)S(1)}, /...) while((s32[]{:T(128)}, bf16[128,64]{1,0:T(8,128)(2,1)S(1)}, ...), condition=%wide.region_6.7_spmd, body=%wide.region_0.6_spmd.sunk | while | flops 138551632 | bytes 3955077 | solution.py:156
  28.5 43.4 %all_gather.24 = bf16[128,2048]{0,1:T(8,128)(2,1)S(1)} all-gather(bf16[128,64]{0,1:T(8,128)(2,1)S(1)} %copy.20), channel_id=1, replica_groups=mesh['pp'=16,'tp'=32] {'tp'}, dimensions={1}, use_global_device_ids=true | all-gather | bytes 540672 | tf_op jit(solution)/shard_map/while/body/eval_jaxpr/all_gather | solution.py:117
  73.3 1.4 while.60
  75.0 2.8 collective-permute-start
  79.0 29.1 %all_gather.24 = bf16[128,2048]{0,1:T(8,128)(2,1)S(1)} all-gather(bf16[128,64]{0,1:T(8,128)(2,1)S(1)} %copy.20), channel_id=1, replica_groups=mesh['pp'=16,'tp'=32] {'tp'}, dimensions={1}, use_global_device_ids=true | all-gather | bytes 540672 | tf_op jit(solution)/shard_map/while/body/eval_jaxpr/all_gather | solution.py:117
  109.5 1.4 while.60
  111.2 3.9 collective-permute-start
  116.3 31.0 %all_gather.24 = bf16[128,2048]{0,1:T(8,128)(2,1)S(1)} all-gather(bf16[128,64]{0,1:T(8,128)(2,1)S(1)} %copy.20), channel_id=1, replica_groups=mesh['pp'=16,'tp'=32] {'tp'}, dimensions={1}, use_global_device_ids=true | all-gather | bytes 540672 | tf_op jit(solution)/shard_map/while/body/eval_jaxpr/all_gather | solution.py:117
  148.8 1.4 while.60
  150.5 3.9 collective-permute-start
  155.6 29.1 %all_gather.24 = bf16[128,2048]{0,1:T(8,128)(2,1)S(1)} all-gather(bf16[128,64]{0,1:T(8,128)(2,1)S(1)} %copy.20), channel_id=1, replica_groups=mesh['pp'=16,'tp'=32] {'tp'}, dimensions={1}, use_global_device_ids=true | all-gather | bytes 540672 | tf_op jit(solution)/shard_map/while/body/eval_jaxpr/all_gather | solution.py:117
  186.1 1.4 while.60
  187.8 3.9 collective-permute-start
  192.9 31.0 %all_gather.24 = bf16[128,2048]{0,1:T(8,128)(2,1)S(1)} all-gather(bf16[128,64]{0,1:T(8,128)(2,1)S(1)} %copy.20), channel_id=1, replica_groups=mesh['pp'=16,'tp'=32] {'tp'}, dimensions={1}, use_global_device_ids=true | all-gather | bytes 540672 | tf_op jit(solution)/shard_map/while/body/eval_jaxpr/all_gather | solution.py:117
  225.3 1.4 while.60
  227.1 3.9 collective-permute-start
  232.2 29.1 %all_gather.24 = bf16[128,2048]{0,1:T(8,128)(2,1)S(1)} all-gather(bf16[128,64]{0,1:T(8,128)(2,1)S(1)} %copy.20), channel_id=1, replica_groups=mesh['pp'=16,'tp'=32] {'tp'}, dimensions={1}, use_global_device_ids=true | all-gather | bytes 540672 | tf_op jit(solution)/shard_map/while/body/eval_jaxpr/all_gather | solution.py:117
  262.7 1.4 while.60
  264.4 5.3 collective-permute-start
  270.9 31.0 %all_gather.24 = bf16[128,2048]{0,1:T(8,128)(2,1)S(1)} all-gather(bf16[128,64]{0,1:T(8,128)(2,1)S(1)} %copy.20), channel_id=1, replica_groups=mesh['pp'=16,'tp'=32] {'tp'}, dimensions={1}, use_global_device_ids=true | all-gather | bytes 540672 | tf_op jit(solution)/shard_map/while/body/eval_jaxpr/all_gather | solution.py:117
  303.3 1.4 while.60
  305.0 6.1 collective-permute-start
  312.2 29.1 %all_gather.24 = bf16[128,2048]{0,1:T(8,128)(2,1)S(1)} all-gather(bf16[128,64]{0,1:T(8,128)(2,1)S(1)} %copy.20), channel_id=1, replica_groups=mesh['pp'=16,'tp'=32] {'tp'}, dimensions={1}, use_global_device_ids=true | all-gather | bytes 540672 | tf_op jit(solution)/shard_map/while/body/eval_jaxpr/all_gather | solution.py:117
  342.7 1.4 while.60
  344.5 6.0 collective-permute-start
  351.7 31.0 %all_gather.24 = bf16[128,2048]{0,1:T(8,128)(2,1)S(1)} all-gather(bf16[128,64]{0,1:T(8,128)(2,1)S(1)} %copy.20), channel_id=1, replica_groups=mesh['pp'=16,'tp'=32] {'tp'}, dimensions={1}, use_global_device_ids=true | all-gather | bytes 540672 | tf_op jit(solution)/shard_map/while/body/eval_jaxpr/all_gather | solution.py:117
  385.8 6.1 collective-permute-start
  393.0 29.1 %all_gather.24 = bf16[128,2048]{0,1:T(8,128)(2,1)S(1)} all-gather(bf16[128,64]{0,1:T(8,128)(2,1)S(1)} %copy.20), channel_id=1, replica_groups=mesh['pp'=16,'tp'=32] {'tp'}, dimensions={1}, use_global_device_ids=true | all-gather | bytes 540672 | tf_op jit(solution)/shard_map/while/body/eval_jaxpr/all_gather | solution.py:117
  423.5 1.4 while.60
  425.3 6.1 collective-permute-start
  432.5 31.0 %all_gather.24 = bf16[128,2048]{0,1:T(8,128)(2,1)S(1)} all-gather(bf16[128,64]{0,1:T(8,128)(2,1)S(1)} %copy.20), channel_id=1, replica_groups=mesh['pp'=16,'tp'=32] {'tp'}, dimensions={1}, use_global_device_ids=true | all-gather | bytes 540672 | tf_op jit(solution)/shard_map/while/body/eval_jaxpr/all_gather | solution.py:117
  466.7 6.0 collective-permute-start
  473.8 29.1 %all_gather.24 = bf16[128,2048]{0,1:T(8,128)(2,1)S(1)} all-gather(bf16[128,64]{0,1:T(8,128)(2,1)S(1)} %copy.20), channel_id=1, replica_groups=mesh['pp'=16,'tp'=32] {'tp'}, dimensions={1}, use_global_device_ids=true | all-gather | bytes 540672 | tf_op jit(solution)/shard_map/while/body/eval_jaxpr/all_gather | solution.py:117
  504.3 1.4 while.60
  506.1 6.1 collective-permute-start
  513.3 31.0 %all_gather.24 = bf16[128,2048]{0,1:T(8,128)(2,1)S(1)} all-gather(bf16[128,64]{0,1:T(8,128)(2,1)S(1)} %copy.20), channel_id=1, replica_groups=mesh['pp'=16,'tp'=32] {'tp'}, dimensions={1}, use_global_device_ids=true | all-gather | bytes 540672 | tf_op jit(solution)/shard_map/while/body/eval_jaxpr/all_gather | solution.py:117
  547.5 6.1 collective-permute-start
  554.6 29.1 %all_gather.24 = bf16[128,2048]{0,1:T(8,128)(2,1)S(1)} all-gather(bf16[128,64]{0,1:T(8,128)(2,1)S(1)} %copy.20), channel_id=1, replica_groups=mesh['pp'=16,'tp'=32] {'tp'}, dimensions={1}, use_global_device_ids=true | all-gather | bytes 540672 | tf_op jit(solution)/shard_map/while/body/eval_jaxpr/all_gather | solution.py:117
  585.1 1.4 while.60
  586.9 6.0 collective-permute-start
  594.1 31.0 %all_gather.24 = bf16[128,2048]{0,1:T(8,128)(2,1)S(1)} all-gather(bf16[128,64]{0,1:T(8,128)(2,1)S(1)} %copy.20), channel_id=1, replica_groups=mesh['pp'=16,'tp'=32] {'tp'}, dimensions={1}, use_global_device_ids=true | all-gather | bytes 540672 | tf_op jit(solution)/shard_map/while/body/eval_jaxpr/all_gather | solution.py:117
  628.3 6.1 collective-permute-start
  635.4 29.1 %all_gather.24 = bf16[128,2048]{0,1:T(8,128)(2,1)S(1)} all-gather(bf16[128,64]{0,1:T(8,128)(2,1)S(1)} %copy.20), channel_id=1, replica_groups=mesh['pp'=16,'tp'=32] {'tp'}, dimensions={1}, use_global_device_ids=true | all-gather | bytes 540672 | tf_op jit(solution)/shard_map/while/body/eval_jaxpr/all_gather | solution.py:117
  667.7 6.1 collective-permute-start
  674.9 31.0 %all_gather.24 = bf16[128,2048]{0,1:T(8,128)(2,1)S(1)} all-gather(bf16[128,64]{0,1:T(8,128)(2,1)S(1)} %copy.20), channel_id=1, replica_groups=mesh['pp'=16,'tp'=32] {'tp'}, dimensions={1}, use_global_device_ids=true | all-gather | bytes 540672 | tf_op jit(solution)/shard_map/while/body/eval_jaxpr/all_gather | solution.py:117
  707.3 1.4 while.60
  709.1 6.0 collective-permute-start
  716.2 29.1 %all_gather.24 = bf16[128,2048]{0,1:T(8,128)(2,1)S(1)} all-gather(bf16[128,64]{0,1:T(8,128)(2,1)S(1)} %copy.20), channel_id=1, replica_groups=mesh['pp'=16,'tp'=32] {'tp'}, dimensions={1}, use_global_device_ids=true | all-gather | bytes 540672 | tf_op jit(solution)/shard_map/while/body/eval_jaxpr/all_gather | solution.py:117
  748.5 6.1 collective-permute-start
  755.7 31.0 %all_gather.24 = bf16[128,2048]{0,1:T(8,128)(2,1)S(1)} all-gather(bf16[128,64]{0,1:T(8,128)(2,1)S(1)} %copy.20), channel_id=1, replica_groups=mesh['pp'=16,'tp'=32] {'tp'}, dimensions={1}, use_global_device_ids=true | all-gather | bytes 540672 | tf_op jit(solution)/shard_map/while/body/eval_jaxpr/all_gather | solution.py:117
  788.1 1.4 while.60
  789.9 6.1 collective-permute-start
  797.0 29.1 %all_gather.24 = bf16[128,2048]{0,1:T(8,128)(2,1)S(1)} all-gather(bf16[128,64]{0,1:T(8,128)(2,1)S(1)} %copy.20), channel_id=1, replica_groups=mesh['pp'=16,'tp'=32] {'tp'}, dimensions={1}, use_global_device_ids=true | all-gather | bytes 540672 | tf_op jit(solution)/shard_map/while/body/eval_jaxpr/all_gather | solution.py:117
  827.5 1.4 while.60
  829.3 6.0 collective-permute-start
  836.5 31.0 %all_gather.24 = bf16[128,2048]{0,1:T(8,128)(2,1)S(1)} all-gather(bf16[128,64]{0,1:T(8,128)(2,1)S(1)} %copy.20), channel_id=1, replica_groups=mesh['pp'=16,'tp'=32] {'tp'}, dimensions={1}, use_global_device_ids=true | all-gather | bytes 540672 | tf_op jit(solution)/shard_map/while/body/eval_jaxpr/all_gather | solution.py:117
  870.7 6.1 collective-permute-start
  877.8 29.1 %all_gather.24 = bf16[128,2048]{0,1:T(8,128)(2,1)S(1)} all-gather(bf16[128,64]{0,1:T(8,128)(2,1)S(1)} %copy.20), channel_id=1, replica_groups=mesh['pp'=16,'tp'=32] {'tp'}, dimensions={1}, use_global_device_ids=true | all-gather | bytes 540672 | tf_op jit(solution)/shard_map/while/body/eval_jaxpr/all_gather | solution.py:117
  910.1 6.1 collective-permute-start
  917.3 31.0 %all_gather.24 = bf16[128,2048]{0,1:T(8,128)(2,1)S(1)} all-gather(bf16[128,64]{0,1:T(8,128)(2,1)S(1)} %copy.20), channel_id=1, replica_groups=mesh['pp'=16,'tp'=32] {'tp'}, dimensions={1}, use_global_device_ids=true | all-gather | bytes 540672 | tf_op jit(solution)/shard_map/while/body/eval_jaxpr/all_gather | solution.py:117
  949.7 1.4 while.60
  951.5 6.0 collective-permute-start
  959.3 72.4 %all-gather.3.cloned.1.call-done = bf16[16384,64]{1,0:T(8,128)(2,1)} async-done(((bf16[1024,64]{1,0:T(8,128)(2,1)}), bf16[16384,64]{1,0:T(8,128)(2,1)}) %all-gather.3.cloned.1.call-update) | async-done | bytes 2097168 | tf_op jit(solution)/shard_map/all_gather | solution.py:18
  (693 shorter events, 112.3 us)
Async XLA Ops:
  6.5 21.7 %copy-start.4 = (f32[1,64]{1,0:T(1,128)S(1)}, f32[1,64]{1,0:T(1,128)}, u32[]{:S(2)}) copy-start(f32[1,64]{1,0:T(1,128)} %param.19) | copy-start | bytes 772
  6.5 21.7 %copy-start.3 = (f32[1,64]{1,0:T(1,128)S(1)}, f32[1,64]{1,0:T(1,128)}, u32[]{:S(2)}) copy-start(f32[1,64]{1,0:T(1,128)} %param.21) | copy-start | bytes 772
  6.5 21.7 %copy-start.2 = (f32[1,128,1]{1,2,0:T(1,128)S(1)}, f32[1,128,1]{1,2,0:T(1,128)}, u32[]{:S(2)}) copy-start(f32[1,128,1]{1,2,0:T(1,128)} %param.20) | copy-start | bytes 1540
  6.5 21.7 %copy-start.1 = (f32[1,2048]{1,0:T(1,128)S(1)}, f32[1,2048]{1,0:T(1,128)}, u32[]{:S(2)}) copy-start(f32[1,2048]{1,0:T(1,128)} %param.14) | copy-start | bytes 24580
  6.5 1025.1 %all-gather.3.cloned.1.call-start = ((), (), s32[]{:S(2)}) async-start(), calls=%async_computation | async-start | bytes 4456448 | tf_op jit(solution)/shard_map/all_gather | solution.py:18
  75.0 3.8 collective-permute-start
  111.2 5.0 collective-permute-start
  150.5 5.0 collective-permute-start
  187.8 5.0 collective-permute-start
  227.1 5.0 collective-permute-start
  264.4 6.3 collective-permute-start
  305.0 7.1 collective-permute-start
  344.5 7.1 collective-permute-start
  385.8 7.1 collective-permute-start
  425.3 7.1 collective-permute-start
  466.7 7.1 collective-permute-start
  506.1 7.1 collective-permute-start
  547.5 7.1 collective-permute-start
  586.9 7.1 collective-permute-start
  628.3 7.1 collective-permute-start
  667.7 7.1 collective-permute-start
  709.1 7.1 collective-permute-start
  748.5 7.1 collective-permute-start
  789.9 7.1 collective-permute-start
  829.3 7.1 collective-permute-start
  870.7 7.1 collective-permute-start
  910.1 7.1 collective-permute-start
  951.5 7.1 collective-permute-start
  958.5 0.7 copy-start
Sparse Core Ops, SparseCore 0:
  959.4 72.2 all-gather.2
where the time goes:
time: 1040 us
  blocking collectives  724 us (70%)
  starting transfers between devices  127 us (12%)
  waiting for transfers between devices  95.4 us (9%)
  matrix products  47.4 us (5%)
  other arithmetic  23.2 us (2%)
  between operations  13.5 us (1%)
    all_gather x23, blocking collectives, one_step(): lax.all_gather(current, 'tp', axis=1, tiled=True)  704 us
    ppermute x23, starting transfers between devices, shifted(): return lax.ppermute(array, axis, pairs)  127 us
    all_gather x1, waiting for transfers between devices, from_root(): lax.all_gather(array, axis)  72.4 us
    ppermute x23, waiting for transfers between devices, shifted(): return lax.ppermute(array, axis, pairs)  23 us
  transfers between devices with their start and end apart: 24, of which 24 were waited for; matrix products, arithmetic and copies ran while one was open for 0% of the time, Pallas kernels for 0%

commit v1 on v0

--- a/solution.py
+++ b/solution.py
@@ -2,6 +2,7 @@
 import jax.numpy as jnp
 from jax import lax
 from jax.sharding import PartitionSpec as P
+from jax.lax import all_to_all, axis_size
 
 HEAD = 64
 SEG = 64
@@ -114,7 +115,14 @@
         first_slot = jnp.clip(step_index, 0, unit_count - 1)
         fresh_rows = lax.dynamic_slice_in_dim(entering, first_slot * seq_len, seq_len, 0)
         current = jnp.where(layer_ordinal == 0, fresh_rows, incoming)
-        projected, squares = add_piece(lax.all_gather(current, "tp", axis=1, tiled=True))
+        projected, squares = add_piece(
+            jnp.concatenate(
+                all_to_all(
+                    jnp.stack([current for _ in range(axis_size("tp"))], axis=0), "tp", 0, 0
+                ),
+                1,
+            )
+        )
         inverse = lax.rsqrt(squares / model_width + EPSILON)[:, None]
         projected = projected * inverse
 

time: 1040 us -> 1260 us (1.21)
  waiting for transfers between devices: 95.4 us -> 861 us
  blocking collectives: 724 us -> 19.7 us
  starting transfers between devices: 127 us -> 262 us
  local copies, waits for them, and re-layouts: 7.26 us -> 28.5 us
    all_to_all x0 -> x23, waiting for transfers between devices: none -> 770 us  [one_step(): all_to_all(jnp.stack([current for _ in range(axis_size('tp'))], axis=0),...]
    all_gather x23 -> x0, blocking collectives: 704 us -> none  [one_step(): lax.all_gather(current, 'tp', axis=1, tiled=True)]
    all_to_all x0 -> x23, starting transfers between devices: none -> 135 us  [one_step(): all_to_all(jnp.stack([current for _ in range(axis_size('tp'))], axis=0),...]
    another operation x0 -> x23, local copies, waits for them, and re-layouts: none -> 21.2 us  [one_step(): jnp.stack([current for _ in range(axis_size('tp'))], axis=0)]
  transfers between devices with their start and end apart: 24 -> 47, of which waited for: 24 -> 47; matrix products, arithmetic and copies ran while one was open for 0% -> 0% of each run, Pallas kernels for 0% -> 0%
where the time goes in v1:
time: 1260 us
  waiting for transfers between devices  861 us (68%)
  starting transfers between devices  262 us (21%)
  matrix products  37.8 us (3%)
  other arithmetic  31.1 us (2%)
  local copies, waits for them, and re-layouts  28.5 us (2%)
  blocking collectives  19.7 us (2%)
  between operations  13.5 us (1%)
    all_to_all x23, waiting for transfers between devices, one_step(): all_to_all(jnp.stack([current for _ in range(axis_size('tp'))], axis=0),...  770 us
    all_to_all x23, starting transfers between devices, one_step(): all_to_all(jnp.stack([current for _ in range(axis_size('tp'))], axis=0),...  135 us
    ppermute x23, starting transfers between devices, shifted(): return lax.ppermute(array, axis, pairs)  127 us
    all_gather x1, waiting for transfers between devices, from_root(): lax.all_gather(array, axis)  68.2 us
  transfers between devices with their start and end apart: 47, of which 47 were waited for; matrix products, arithmetic and copies ran while one was open for 0% of the time, Pallas kernels for 0%

profile of v1, /device:TPU:1, one launch (start us, length us, event | category | flops | bytes accessed | tf_op | source)
XLA Modules:
  0.0 1257.2 jit_solution(15405859471785468717)
XLA Ops:
  7.3 19.7 %all_gather.9 = bf16[1024,64]{1,0:T(8,128)(2,1)S(1)} all-gather(bf16[64,64]{1,0:T(8,128)(2,1)} %param.13), channel_id=1, replica_groups=mesh['pp'=16,'tp'=32] {'pp'}, dimensions={0}, use_global_device_ids=true | all-gather | bytes 139264 | tf_op jit(solution)/shard_map/all_gather | solution.py:89
  28.3 1151.4 %while.59 = (s32[]{:T(128)}, bf16[128,64]{1,0:T(8,128)(2,1)S(1)}, bf16[1024,64]{1,0:T(8,128)(2,1)S(1)}, pred[]{:T(512)}, bf16[1024,64]{1,0:T(8,128)(2,1)S(1)}, /...) while((s32[]{:T(128)}, bf16[128,64]{1,0:T(8,128)(2,1)S(1)}, ...), condition=%wide.region_6.7_spmd, body=%wide.region_0.6_spmd.sunk | while | flops 138551632 | bytes 6576549 | solution.py:164
  29.4 21.1 %all-to-all-start = ((bf16[32,128,64]{1,2,0:T(8,128)(2,1)}), bf16[32,128,64]{1,2,0:T(8,128)(2,1)S(1)}, u32[]{:S(2)}, u32[]{:S(2)}) async-start(bf16[32,128,64]{1,2,0:T(8,128)(2,1)} %stack.7), calls=%async_computation | async-start | bytes 1048576 | tf_op jit(solution)/shard_map/while/body/eval_jaxpr/all_to_all | solution.py:120
  50.6 33.5 %all-to-all-done = bf16[32,128,64]{1,2,0:T(8,128)(2,1)S(1)} async-done(((bf16[32,128,64]{1,2,0:T(8,128)(2,1)}), bf16[32,128,64]{1,2,0:T(8,128)(2,1)S(1)}, u32[]{:S(2)}, u32[]{:S(2)}) %all-to-all-start) | async-done | bytes 524320 | tf_op jit(solution)/shard_map/while/body/eval_jaxpr/all_to_all | solution.py:120
  97.0 33.5 %all-to-all-done = bf16[32,128,64]{1,2,0:T(8,128)(2,1)S(1)} async-done(((bf16[32,128,64]{1,2,0:T(8,128)(2,1)}), bf16[32,128,64]{1,2,0:T(8,128)(2,1)S(1)}, u32[]{:S(2)}, u32[]{:S(2)}) %all-to-all-start) | async-done | bytes 524320 | tf_op jit(solution)/shard_map/while/body/eval_jaxpr/all_to_all | solution.py:120
  139.5 5.2 all-to-all-start
  144.8 33.5 %all-to-all-done = bf16[32,128,64]{1,2,0:T(8,128)(2,1)S(1)} async-done(((bf16[32,128,64]{1,2,0:T(8,128)(2,1)}), bf16[32,128,64]{1,2,0:T(8,128)(2,1)S(1)}, u32[]{:S(2)}, u32[]{:S(2)}) %all-to-all-start) | async-done | bytes 524320 | tf_op jit(solution)/shard_map/while/body/eval_jaxpr/all_to_all | solution.py:120
  192.6 33.5 %all-to-all-done = bf16[32,128,64]{1,2,0:T(8,128)(2,1)S(1)} async-done(((bf16[32,128,64]{1,2,0:T(8,128)(2,1)}), bf16[32,128,64]{1,2,0:T(8,128)(2,1)S(1)}, u32[]{:S(2)}, u32[]{:S(2)}) %all-to-all-start) | async-done | bytes 524320 | tf_op jit(solution)/shard_map/while/body/eval_jaxpr/all_to_all | solution.py:120
  235.2 5.2 all-to-all-start
  240.4 33.5 %all-to-all-done = bf16[32,128,64]{1,2,0:T(8,128)(2,1)S(1)} async-done(((bf16[32,128,64]{1,2,0:T(8,128)(2,1)}), bf16[32,128,64]{1,2,0:T(8,128)(2,1)S(1)}, u32[]{:S(2)}, u32[]{:S(2)}) %all-to-all-start) | async-done | bytes 524320 | tf_op jit(solution)/shard_map/while/body/eval_jaxpr/all_to_all | solution.py:120
  283.0 5.2 all-to-all-start
  288.2 33.5 %all-to-all-done = bf16[32,128,64]{1,2,0:T(8,128)(2,1)S(1)} async-done(((bf16[32,128,64]{1,2,0:T(8,128)(2,1)}), bf16[32,128,64]{1,2,0:T(8,128)(2,1)S(1)}, u32[]{:S(2)}, u32[]{:S(2)}) %all-to-all-start) | async-done | bytes 524320 | tf_op jit(solution)/shard_map/while/body/eval_jaxpr/all_to_all | solution.py:120
  324.8 5.3 collective-permute-start
  332.1 5.2 all-to-all-start
  337.4 33.5 %all-to-all-done = bf16[32,128,64]{1,2,0:T(8,128)(2,1)S(1)} async-done(((bf16[32,128,64]{1,2,0:T(8,128)(2,1)}), bf16[32,128,64]{1,2,0:T(8,128)(2,1)S(1)}, u32[]{:S(2)}, u32[]{:S(2)}) %all-to-all-start) | async-done | bytes 524320 | tf_op jit(solution)/shard_map/while/body/eval_jaxpr/all_to_all | solution.py:120
  374.0 6.1 collective-permute-start
  382.1 5.2 all-to-all-start
  387.3 33.5 %all-to-all-done = bf16[32,128,64]{1,2,0:T(8,128)(2,1)S(1)} async-done(((bf16[32,128,64]{1,2,0:T(8,128)(2,1)}), bf16[32,128,64]{1,2,0:T(8,128)(2,1)S(1)}, u32[]{:S(2)}, u32[]{:S(2)}) %all-to-all-start) | async-done | bytes 524320 | tf_op jit(solution)/shard_map/while/body/eval_jaxpr/all_to_all | solution.py:120
  423.9 6.1 collective-permute-start
  432.0 5.2 all-to-all-start
  437.2 33.5 %all-to-all-done = bf16[32,128,64]{1,2,0:T(8,128)(2,1)S(1)} async-done(((bf16[32,128,64]{1,2,0:T(8,128)(2,1)}), bf16[32,128,64]{1,2,0:T(8,128)(2,1)S(1)}, u32[]{:S(2)}, u32[]{:S(2)}) %all-to-all-start) | async-done | bytes 524320 | tf_op jit(solution)/shard_map/while/body/eval_jaxpr/all_to_all | solution.py:120
  473.8 6.1 collective-permute-start
  481.9 5.2 all-to-all-start
  487.2 33.5 %all-to-all-done = bf16[32,128,64]{1,2,0:T(8,128)(2,1)S(1)} async-done(((bf16[32,128,64]{1,2,0:T(8,128)(2,1)}), bf16[32,128,64]{1,2,0:T(8,128)(2,1)S(1)}, u32[]{:S(2)}, u32[]{:S(2)}) %all-to-all-start) | async-done | bytes 524320 | tf_op jit(solution)/shard_map/while/body/eval_jaxpr/all_to_all | solution.py:120
  523.7 6.1 collective-permute-start
  531.8 5.2 all-to-all-start
  537.1 33.5 %all-to-all-done = bf16[32,128,64]{1,2,0:T(8,128)(2,1)S(1)} async-done(((bf16[32,128,64]{1,2,0:T(8,128)(2,1)}), bf16[32,128,64]{1,2,0:T(8,128)(2,1)S(1)}, u32[]{:S(2)}, u32[]{:S(2)}) %all-to-all-start) | async-done | bytes 524320 | tf_op jit(solution)/shard_map/while/body/eval_jaxpr/all_to_all | solution.py:120
  573.7 6.1 collective-permute-start
  581.7 5.2 all-to-all-start
  587.0 33.5 %all-to-all-done = bf16[32,128,64]{1,2,0:T(8,128)(2,1)S(1)} async-done(((bf16[32,128,64]{1,2,0:T(8,128)(2,1)}), bf16[32,128,64]{1,2,0:T(8,128)(2,1)S(1)}, u32[]{:S(2)}, u32[]{:S(2)}) %all-to-all-start) | async-done | bytes 524320 | tf_op jit(solution)/shard_map/while/body/eval_jaxpr/all_to_all | solution.py:120
  623.6 6.1 collective-permute-start
  631.7 5.2 all-to-all-start
  636.9 33.5 %all-to-all-done = bf16[32,128,64]{1,2,0:T(8,128)(2,1)S(1)} async-done(((bf16[32,128,64]{1,2,0:T(8,128)(2,1)}), bf16[32,128,64]{1,2,0:T(8,128)(2,1)S(1)}, u32[]{:S(2)}, u32[]{:S(2)}) %all-to-all-start) | async-done | bytes 524320 | tf_op jit(solution)/shard_map/while/body/eval_jaxpr/all_to_all | solution.py:120
  673.5 6.1 collective-permute-start
  681.6 5.2 all-to-all-start
  686.8 33.5 %all-to-all-done = bf16[32,128,64]{1,2,0:T(8,128)(2,1)S(1)} async-done(((bf16[32,128,64]{1,2,0:T(8,128)(2,1)}), bf16[32,128,64]{1,2,0:T(8,128)(2,1)S(1)}, u32[]{:S(2)}, u32[]{:S(2)}) %all-to-all-start) | async-done | bytes 524320 | tf_op jit(solution)/shard_map/while/body/eval_jaxpr/all_to_all | solution.py:120
  723.4 6.1 collective-permute-start
  731.5 5.2 all-to-all-start
  736.8 33.5 %all-to-all-done = bf16[32,128,64]{1,2,0:T(8,128)(2,1)S(1)} async-done(((bf16[32,128,64]{1,2,0:T(8,128)(2,1)}), bf16[32,128,64]{1,2,0:T(8,128)(2,1)S(1)}, u32[]{:S(2)}, u32[]{:S(2)}) %all-to-all-start) | async-done | bytes 524320 | tf_op jit(solution)/shard_map/while/body/eval_jaxpr/all_to_all | solution.py:120
  773.3 6.1 collective-permute-start
  781.4 5.2 all-to-all-start
  786.7 33.5 %all-to-all-done = bf16[32,128,64]{1,2,0:T(8,128)(2,1)S(1)} async-done(((bf16[32,128,64]{1,2,0:T(8,128)(2,1)}), bf16[32,128,64]{1,2,0:T(8,128)(2,1)S(1)}, u32[]{:S(2)}, u32[]{:S(2)}) %all-to-all-start) | async-done | bytes 524320 | tf_op jit(solution)/shard_map/while/body/eval_jaxpr/all_to_all | solution.py:120
  823.3 6.1 collective-permute-start
  831.3 5.2 all-to-all-start
  836.6 33.5 %all-to-all-done = bf16[32,128,64]{1,2,0:T(8,128)(2,1)S(1)} async-done(((bf16[32,128,64]{1,2,0:T(8,128)(2,1)}), bf16[32,128,64]{1,2,0:T(8,128)(2,1)S(1)}, u32[]{:S(2)}, u32[]{:S(2)}) %all-to-all-start) | async-done | bytes 524320 | tf_op jit(solution)/shard_map/while/body/eval_jaxpr/all_to_all | solution.py:120
  873.2 6.1 collective-permute-start
  881.3 5.2 all-to-all-start
  886.5 33.5 %all-to-all-done = bf16[32,128,64]{1,2,0:T(8,128)(2,1)S(1)} async-done(((bf16[32,128,64]{1,2,0:T(8,128)(2,1)}), bf16[32,128,64]{1,2,0:T(8,128)(2,1)S(1)}, u32[]{:S(2)}, u32[]{:S(2)}) %all-to-all-start) | async-done | bytes 524320 | tf_op jit(solution)/shard_map/while/body/eval_jaxpr/all_to_all | solution.py:120
  923.1 6.1 collective-permute-start
  931.2 5.2 all-to-all-start
  936.4 33.5 %all-to-all-done = bf16[32,128,64]{1,2,0:T(8,128)(2,1)S(1)} async-done(((bf16[32,128,64]{1,2,0:T(8,128)(2,1)}), bf16[32,128,64]{1,2,0:T(8,128)(2,1)S(1)}, u32[]{:S(2)}, u32[]{:S(2)}) %all-to-all-start) | async-done | bytes 524320 | tf_op jit(solution)/shard_map/while/body/eval_jaxpr/all_to_all | solution.py:120
  973.0 6.1 collective-permute-start
  981.1 5.2 all-to-all-start
  986.4 33.5 %all-to-all-done = bf16[32,128,64]{1,2,0:T(8,128)(2,1)S(1)} async-done(((bf16[32,128,64]{1,2,0:T(8,128)(2,1)}), bf16[32,128,64]{1,2,0:T(8,128)(2,1)S(1)}, u32[]{:S(2)}, u32[]{:S(2)}) %all-to-all-start) | async-done | bytes 524320 | tf_op jit(solution)/shard_map/while/body/eval_jaxpr/all_to_all | solution.py:120
  1022.9 6.1 collective-permute-start
  1031.0 5.2 all-to-all-start
  1036.3 33.5 %all-to-all-done = bf16[32,128,64]{1,2,0:T(8,128)(2,1)S(1)} async-done(((bf16[32,128,64]{1,2,0:T(8,128)(2,1)}), bf16[32,128,64]{1,2,0:T(8,128)(2,1)S(1)}, u32[]{:S(2)}, u32[]{:S(2)}) %all-to-all-start) | async-done | bytes 524320 | tf_op jit(solution)/shard_map/while/body/eval_jaxpr/all_to_all | solution.py:120
  1072.9 6.1 collective-permute-start
  1080.9 5.2 all-to-all-start
  1086.2 33.5 %all-to-all-done = bf16[32,128,64]{1,2,0:T(8,128)(2,1)S(1)} async-done(((bf16[32,128,64]{1,2,0:T(8,128)(2,1)}), bf16[32,128,64]{1,2,0:T(8,128)(2,1)S(1)}, u32[]{:S(2)}, u32[]{:S(2)}) %all-to-all-start) | async-done | bytes 524320 | tf_op jit(solution)/shard_map/while/body/eval_jaxpr/all_to_all | solution.py:120
  1122.8 6.1 collective-permute-start
  1136.1 33.5 %all-to-all-done = bf16[32,128,64]{1,2,0:T(8,128)(2,1)S(1)} async-done(((bf16[32,128,64]{1,2,0:T(8,128)(2,1)}), bf16[32,128,64]{1,2,0:T(8,128)(2,1)S(1)}, u32[]{:S(2)}, u32[]{:S(2)}) %all-to-all-start) | async-done | bytes 524320 | tf_op jit(solution)/shard_map/while/body/eval_jaxpr/all_to_all | solution.py:120
  1172.7 6.1 collective-permute-start
  1180.5 68.2 %all-gather.3.cloned.1.call-done = bf16[16384,64]{1,0:T(8,128)(2,1)} async-done(((bf16[1024,64]{1,0:T(8,128)(2,1)}), bf16[16384,64]{1,0:T(8,128)(2,1)}) %all-gather.3.cloned.1.call-update) | async-done | bytes 2097168 | tf_op jit(solution)/shard_map/all_gather | solution.py:19
  (762 shorter events, 187.1 us)
Async XLA Ops:
  6.5 21.8 %copy-start.4 = (f32[1,64]{1,0:T(1,128)S(1)}, f32[1,64]{1,0:T(1,128)}, u32[]{:S(2)}) copy-start(f32[1,64]{1,0:T(1,128)} %param.19) | copy-start | bytes 772
  6.5 21.8 %copy-start.3 = (f32[1,64]{1,0:T(1,128)S(1)}, f32[1,64]{1,0:T(1,128)}, u32[]{:S(2)}) copy-start(f32[1,64]{1,0:T(1,128)} %param.21) | copy-start | bytes 772
  6.5 21.8 %copy-start.2 = (f32[1,128,1]{1,2,0:T(1,128)S(1)}, f32[1,128,1]{1,2,0:T(1,128)}, u32[]{:S(2)}) copy-start(f32[1,128,1]{1,2,0:T(1,128)} %param.20) | copy-start | bytes 1540
  6.5 21.8 %copy-start.1 = (f32[1,2048]{1,0:T(1,128)S(1)}, f32[1,2048]{1,0:T(1,128)}, u32[]{:S(2)}) copy-start(f32[1,2048]{1,0:T(1,128)} %param.14) | copy-start | bytes 24580
  6.5 1242.2 %all-gather.3.cloned.1.call-start = ((), (), s32[]{:S(2)}) async-start(), calls=%async_computation.1 | async-start | bytes 4456448 | tf_op jit(solution)/shard_map/all_gather | solution.py:19
  29.4 54.7 %all-to-all-start = ((bf16[32,128,64]{1,2,0:T(8,128)(2,1)}), bf16[32,128,64]{1,2,0:T(8,128)(2,1)S(1)}, u32[]{:S(2)}, u32[]{:S(2)}) async-start(bf16[32,128,64]{1,2,0:T(8,128)(2,1)} %stack.7), calls=%async_computation | async-start | bytes 1048576 | tf_op jit(solution)/shard_map/while/body/eval_jaxpr/all_to_all | solution.py:120
  87.1 3.8 collective-permute-start
  92.0 38.4 %all-to-all-start = ((bf16[32,128,64]{1,2,0:T(8,128)(2,1)}), bf16[32,128,64]{1,2,0:T(8,128)(2,1)S(1)}, u32[]{:S(2)}, u32[]{:S(2)}) async-start(bf16[32,128,64]{1,2,0:T(8,128)(2,1)} %stack.7), calls=%async_computation | async-start | bytes 1048576 | tf_op jit(solution)/shard_map/while/body/eval_jaxpr/all_to_all | solution.py:120
  133.6 5.0 collective-permute-start
  139.5 38.7 %all-to-all-start = ((bf16[32,128,64]{1,2,0:T(8,128)(2,1)}), bf16[32,128,64]{1,2,0:T(8,128)(2,1)S(1)}, u32[]{:S(2)}, u32[]{:S(2)}) async-start(bf16[32,128,64]{1,2,0:T(8,128)(2,1)} %stack.7), calls=%async_computation | async-start | bytes 1048576 | tf_op jit(solution)/shard_map/while/body/eval_jaxpr/all_to_all | solution.py:120
  181.4 5.0 collective-permute-start
  187.3 38.7 %all-to-all-start = ((bf16[32,128,64]{1,2,0:T(8,128)(2,1)}), bf16[32,128,64]{1,2,0:T(8,128)(2,1)S(1)}, u32[]{:S(2)}, u32[]{:S(2)}) async-start(bf16[32,128,64]{1,2,0:T(8,128)(2,1)} %stack.7), calls=%async_computation | async-start | bytes 1048576 | tf_op jit(solution)/shard_map/while/body/eval_jaxpr/all_to_all | solution.py:120
  229.2 5.0 collective-permute-start
  235.2 38.7 %all-to-all-start = ((bf16[32,128,64]{1,2,0:T(8,128)(2,1)}), bf16[32,128,64]{1,2,0:T(8,128)(2,1)S(1)}, u32[]{:S(2)}, u32[]{:S(2)}) async-start(bf16[32,128,64]{1,2,0:T(8,128)(2,1)} %stack.7), calls=%async_computation | async-start | bytes 1048576 | tf_op jit(solution)/shard_map/while/body/eval_jaxpr/all_to_all | solution.py:120
  277.0 5.0 collective-permute-start
  283.0 38.7 %all-to-all-start = ((bf16[32,128,64]{1,2,0:T(8,128)(2,1)}), bf16[32,128,64]{1,2,0:T(8,128)(2,1)S(1)}, u32[]{:S(2)}, u32[]{:S(2)}) async-start(bf16[32,128,64]{1,2,0:T(8,128)(2,1)} %stack.7), calls=%async_computation | async-start | bytes 1048576 | tf_op jit(solution)/shard_map/while/body/eval_jaxpr/all_to_all | solution.py:120
  324.8 6.3 collective-permute-start
  332.1 38.7 %all-to-all-start = ((bf16[32,128,64]{1,2,0:T(8,128)(2,1)}), bf16[32,128,64]{1,2,0:T(8,128)(2,1)S(1)}, u32[]{:S(2)}, u32[]{:S(2)}) async-start(bf16[32,128,64]{1,2,0:T(8,128)(2,1)} %stack.7), calls=%async_computation | async-start | bytes 1048576 | tf_op jit(solution)/shard_map/while/body/eval_jaxpr/all_to_all | solution.py:120
  374.0 7.1 collective-permute-start
  382.1 38.7 %all-to-all-start = ((bf16[32,128,64]{1,2,0:T(8,128)(2,1)}), bf16[32,128,64]{1,2,0:T(8,128)(2,1)S(1)}, u32[]{:S(2)}, u32[]{:S(2)}) async-start(bf16[32,128,64]{1,2,0:T(8,128)(2,1)} %stack.7), calls=%async_computation | async-start | bytes 1048576 | tf_op jit(solution)/shard_map/while/body/eval_jaxpr/all_to_all | solution.py:120
  423.9 7.1 collective-permute-start
  432.0 38.7 %all-to-all-start = ((bf16[32,128,64]{1,2,0:T(8,128)(2,1)}), bf16[32,128,64]{1,2,0:T(8,128)(2,1)S(1)}, u32[]{:S(2)}, u32[]{:S(2)}) async-start(bf16[32,128,64]{1,2,0:T(8,128)(2,1)} %stack.7), calls=%async_computation | async-start | bytes 1048576 | tf_op jit(solution)/shard_map/while/body/eval_jaxpr/all_to_all | solution.py:120
  473.8 7.1 collective-permute-start
  481.9 38.7 %all-to-all-start = ((bf16[32,128,64]{1,2,0:T(8,128)(2,1)}), bf16[32,128,64]{1,2,0:T(8,128)(2,1)S(1)}, u32[]{:S(2)}, u32[]{:S(2)}) async-start(bf16[32,128,64]{1,2,0:T(8,128)(2,1)} %stack.7), calls=%async_computation | async-start | bytes 1048576 | tf_op jit(solution)/shard_map/while/body/eval_jaxpr/all_to_all | solution.py:120
  523.7 7.1 collective-permute-start
  531.8 38.7 %all-to-all-start = ((bf16[32,128,64]{1,2,0:T(8,128)(2,1)}), bf16[32,128,64]{1,2,0:T(8,128)(2,1)S(1)}, u32[]{:S(2)}, u32[]{:S(2)}) async-start(bf16[32,128,64]{1,2,0:T(8,128)(2,1)} %stack.7), calls=%async_computation | async-start | bytes 1048576 | tf_op jit(solution)/shard_map/while/body/eval_jaxpr/all_to_all | solution.py:120
  573.7 7.1 collective-permute-start
  581.7 38.7 %all-to-all-start = ((bf16[32,128,64]{1,2,0:T(8,128)(2,1)}), bf16[32,128,64]{1,2,0:T(8,128)(2,1)S(1)}, u32[]{:S(2)}, u32[]{:S(2)}) async-start(bf16[32,128,64]{1,2,0:T(8,128)(2,1)} %stack.7), calls=%async_computation | async-start | bytes 1048576 | tf_op jit(solution)/shard_map/while/body/eval_jaxpr/all_to_all | solution.py:120
  623.6 7.1 collective-permute-start
  631.7 38.7 %all-to-all-start = ((bf16[32,128,64]{1,2,0:T(8,128)(2,1)}), bf16[32,128,64]{1,2,0:T(8,128)(2,1)S(1)}, u32[]{:S(2)}, u32[]{:S(2)}) async-start(bf16[32,128,64]{1,2,0:T(8,128)(2,1)} %stack.7), calls=%async_computation | async-start | bytes 1048576 | tf_op jit(solution)/shard_map/while/body/eval_jaxpr/all_to_all | solution.py:120
  673.5 7.1 collective-permute-start
  681.6 38.7 %all-to-all-start = ((bf16[32,128,64]{1,2,0:T(8,128)(2,1)}), bf16[32,128,64]{1,2,0:T(8,128)(2,1)S(1)}, u32[]{:S(2)}, u32[]{:S(2)}) async-start(bf16[32,128,64]{1,2,0:T(8,128)(2,1)} %stack.7), calls=%async_computation | async-start | bytes 1048576 | tf_op jit(solution)/shard_map/while/body/eval_jaxpr/all_to_all | solution.py:120
  723.4 7.1 collective-permute-start
  731.5 38.7 %all-to-all-start = ((bf16[32,128,64]{1,2,0:T(8,128)(2,1)}), bf16[32,128,64]{1,2,0:T(8,128)(2,1)S(1)}, u32[]{:S(2)}, u32[]{:S(2)}) async-start(bf16[32,128,64]{1,2,0:T(8,128)(2,1)} %stack.7), calls=%async_computation | async-start | bytes 1048576 | tf_op jit(solution)/shard_map/while/body/eval_jaxpr/all_to_all | solution.py:120
  773.3 7.1 collective-permute-start
  781.4 38.7 %all-to-all-start = ((bf16[32,128,64]{1,2,0:T(8,128)(2,1)}), bf16[32,128,64]{1,2,0:T(8,128)(2,1)S(1)}, u32[]{:S(2)}, u32[]{:S(2)}) async-start(bf16[32,128,64]{1,2,0:T(8,128)(2,1)} %stack.7), calls=%async_computation | async-start | bytes 1048576 | tf_op jit(solution)/shard_map/while/body/eval_jaxpr/all_to_all | solution.py:120
  823.3 7.1 collective-permute-start
  831.3 38.7 %all-to-all-start = ((bf16[32,128,64]{1,2,0:T(8,128)(2,1)}), bf16[32,128,64]{1,2,0:T(8,128)(2,1)S(1)}, u32[]{:S(2)}, u32[]{:S(2)}) async-start(bf16[32,128,64]{1,2,0:T(8,128)(2,1)} %stack.7), calls=%async_computation | async-start | bytes 1048576 | tf_op jit(solution)/shard_map/while/body/eval_jaxpr/all_to_all | solution.py:120
  873.2 7.1 collective-permute-start
  881.3 38.7 %all-to-all-start = ((bf16[32,128,64]{1,2,0:T(8,128)(2,1)}), bf16[32,128,64]{1,2,0:T(8,128)(2,1)S(1)}, u32[]{:S(2)}, u32[]{:S(2)}) async-start(bf16[32,128,64]{1,2,0:T(8,128)(2,1)} %stack.7), calls=%async_computation | async-start | bytes 1048576 | tf_op jit(solution)/shard_map/while/body/eval_jaxpr/all_to_all | solution.py:120
  923.1 7.1 collective-permute-start
  931.2 38.7 %all-to-all-start = ((bf16[32,128,64]{1,2,0:T(8,128)(2,1)}), bf16[32,128,64]{1,2,0:T(8,128)(2,1)S(1)}, u32[]{:S(2)}, u32[]{:S(2)}) async-start(bf16[32,128,64]{1,2,0:T(8,128)(2,1)} %stack.7), calls=%async_computation | async-start | bytes 1048576 | tf_op jit(solution)/shard_map/while/body/eval_jaxpr/all_to_all | solution.py:120
  973.0 7.1 collective-permute-start
  981.1 38.7 %all-to-all-start = ((bf16[32,128,64]{1,2,0:T(8,128)(2,1)}), bf16[32,128,64]{1,2,0:T(8,128)(2,1)S(1)}, u32[]{:S(2)}, u32[]{:S(2)}) async-start(bf16[32,128,64]{1,2,0:T(8,128)(2,1)} %stack.7), calls=%async_computation | async-start | bytes 1048576 | tf_op jit(solution)/shard_map/while/body/eval_jaxpr/all_to_all | solution.py:120
  1022.9 7.1 collective-permute-start
  1031.0 38.7 %all-to-all-start = ((bf16[32,128,64]{1,2,0:T(8,128)(2,1)}), bf16[32,128,64]{1,2,0:T(8,128)(2,1)S(1)}, u32[]{:S(2)}, u32[]{:S(2)}) async-start(bf16[32,128,64]{1,2,0:T(8,128)(2,1)} %stack.7), calls=%async_computation | async-start | bytes 1048576 | tf_op jit(solution)/shard_map/while/body/eval_jaxpr/all_to_all | solution.py:120
  1072.9 7.1 collective-permute-start
  1080.9 38.7 %all-to-all-start = ((bf16[32,128,64]{1,2,0:T(8,128)(2,1)}), bf16[32,128,64]{1,2,0:T(8,128)(2,1)S(1)}, u32[]{:S(2)}, u32[]{:S(2)}) async-start(bf16[32,128,64]{1,2,0:T(8,128)(2,1)} %stack.7), calls=%async_computation | async-start | bytes 1048576 | tf_op jit(solution)/shard_map/while/body/eval_jaxpr/all_to_all | solution.py:120
  1122.8 7.1 collective-permute-start
  1130.9 38.7 %all-to-all-start = ((bf16[32,128,64]{1,2,0:T(8,128)(2,1)}), bf16[32,128,64]{1,2,0:T(8,128)(2,1)S(1)}, u32[]{:S(2)}, u32[]{:S(2)}) async-start(bf16[32,128,64]{1,2,0:T(8,128)(2,1)} %stack.7), calls=%async_computation | async-start | bytes 1048576 | tf_op jit(solution)/shard_map/while/body/eval_jaxpr/all_to_all | solution.py:120
  1172.7 7.1 collective-permute-start
  1179.8 0.7 copy-start
Sparse Core Ops, SparseCore 0:
  1180.6 68.0 all-gather.2
